TPU v7x, 32 devices: a whole 2x2x4 slice. The times are simulated.
32 devices in a mesh: sp: 8 (over z, y), tp: 4 (over x, core).
Axes of the slice: x: 2, y: 2, z: 4, core: 2. Of those that a mesh axis runs over, the one named last changes fastest.
Arguments:
- tokens: bfloat16 [2048, 4096], P(('sp', 'tp')), may hold values from -700 to 700
- down_query: bfloat16 [4096, 1024], replicated, may hold values from -0.09375 to 0.09375
- down_latent: bfloat16 [4096, 512], replicated, may hold values from -0.09375 to 0.09375
- down_rotary: bfloat16 [4096, 64], replicated, may hold values from -0.09375 to 0.09375
- query_gain: float32 [1024], replicated, may hold values from 0.1 to 1.9
- latent_gain: float32 [512], replicated, may hold values from 0.1 to 1.9
- up_query: bfloat16 [1024, 2048], P(None, 'tp'), may hold values from -0.1875 to 0.1875
- up_query_rotary: bfloat16 [1024, 1024], P(None, 'tp'), may hold values from -0.1875 to 0.1875
- up_key: bfloat16 [512, 2048], P(None, 'tp'), may hold values from -0.25 to 0.25
- up_value: bfloat16 [512, 2048], P(None, 'tp'), may hold values from -0.25 to 0.25
- out_weight: bfloat16 [2048, 4096], P('tp'), may hold values from -0.39648438 to 0.39648438
Outputs:
- mixed: bfloat16 [2048, 4096], P(('sp', 'tp'))
All inputs are finite; a program needn't handle non-finite values.
Results may differ from a plain program's by a relative error of at most 0.03.
Values may be sent and summed in bfloat16 or wider, within the bound.
A program may use at most 192 MiB of HBM per device.

v0:
```python
import functools

import jax
import jax.numpy as jnp
import numpy as np
from jax import lax
from jax.experimental import pallas as pl
from jax.experimental.pallas import tpu as pltpu
from jax.sharding import PartitionSpec as P

NOPE = 128
ROPE = 64
VDIM = 128
LANES = 128

rope_base = 500000.0
norm_eps = 1e-06
masked_score = -1e30
log2e = 1.4426950408889634

MESH = pl.DeviceIdType.MESH
F32 = jnp.float32
BF16 = jnp.bfloat16


def dot(a, b):
    return jnp.dot(a, b, preferred_element_type=F32)


def dot_nt(a, b):
    return lax.dot_general(a, b, (((1,), (1,)), ((), ())), preferred_element_type=F32)


def turn(v, cosine, sine):
    lane = lax.broadcasted_iota(jnp.int32, v.shape, 1)
    other = jnp.where(lane % ROPE < ROPE // 2, pltpu.roll(v, LANES - ROPE // 2, 1), pltpu.roll(v, ROPE // 2, 1))
    return v * cosine + other * sine


def normed(v, gain):
    return v * lax.rsqrt(jnp.mean(v * v, axis=-1, keepdims=True) + norm_eps) * gain


def kernel(
    S,
    T,
    chunks,
    pieces,
    tokens_hbm,
    dq_hbm,
    dl_hbm,
    dr_hbm,
    qg_ref,
    lg_ref,
    uq_hbm,
    ur_hbm,
    uk_hbm,
    uv_hbm,
    ow_hbm,
    base_cos,
    base_sin,
    row_cos,
    row_sin,
    out_ref,
    tokens,
    dq,
    dl,
    dr,
    uq,
    ur,
    uk,
    uv,
    ow,
    kv,
    ql,
    qh,
    acc,
    best,
    att,
    pair_out,
    pair_in,
    kept,
    cross_out,
    cross_in,
    uvt,
    first_keys,
    first_values,
    cos_ref,
    sin_ref,
    load_sem,
    kv_send,
    kv_recv,
    q_send,
    q_recv,
    pair_send,
    pair_recv,
    cross_send,
    cross_recv,
):
    O = S // 2
    rows = tokens.shape[0]
    span = rows * T
    depth = tokens.shape[1]
    heads = qh.shape[0]
    rank = dl.shape[1]
    sp = lax.axis_index("sp")
    tp = lax.axis_index("tp")
    o, i = sp // 2, sp % 2
    g, c = tp // 2, tp % 2

    def dev(o_, i_, g_, c_):
        return {"sp": o_ * 2 + i_, "tp": g_ * 2 + c_}

    across = dev(o, i, 1 - g, c)
    beside = dev(o, 1 - i, g, c)
    mate = dev(o, i, g, 1 - c)

    step = depth // chunks
    loads = []

    def load(src, dst):
        copy = pltpu.make_async_copy(src, dst, load_sem.at[len(loads)])
        loads.append(copy)
        copy.start()
        return copy

    tok_load = load(tokens_hbm, tokens)
    dl_loads = [load(dl_hbm.at[pl.ds(k * step, step)], dl.at[pl.ds(k * step, step)]) for k in range(chunks)]
    dr_load = load(dr_hbm, dr)
    dq_loads = [load(dq_hbm.at[pl.ds(k * step, step)], dq.at[pl.ds(k * step, step)]) for k in range(chunks)]
    up_loads = [load(uq_hbm, uq), load(ur_hbm, ur), load(uk_hbm, uk), load(uv_hbm, uv)]
    ow_load = load(ow_hbm, ow)

    barrier = pltpu.get_barrier_semaphore()
    for d in range(1, O):
        pl.semaphore_signal(barrier, inc=1, device_id=dev((o + d) % O, i, g, c), device_id_type=MESH)
    for target in (across, beside, mate):
        pl.semaphore_signal(barrier, inc=1, device_id=target, device_id_type=MESH)

    def block(o_, i_, g_, c_):
        return (o_ * 2 + i_) * T + g_ * 2 + c_

    def block_rows(b):
        return pl.ds(pl.multiple_of(b * rows, rows), rows)

    def kv_copy(b, target, index):
        part = kv.at[block_rows(b)]
        return pltpu.make_async_remote_copy(
            src_ref=part,
            dst_ref=part,
            send_sem=kv_send.at[index],
            recv_sem=kv_recv.at[b],
            device_id=target,
            device_id_type=MESH,
        )

    def kv_wait(b):
        kv_copy(b, mate, 0).wait_recv()

    start_cos, start_sin = base_cos[pl.ds(sp, 1), :], base_sin[pl.ds(sp, 1), :]
    sign = jnp.where(lax.broadcasted_iota(jnp.int32, (1, LANES), 1) % ROPE < ROPE // 2, -1.0, 1.0)
    cos_ref[...] = start_cos * row_cos[...] - start_sin * row_sin[...]
    sin_ref[...] = (start_sin * row_cos[...] + start_cos * row_sin[...]) * sign

    tok_load.wait()
    latent = jnp.zeros((rows, rank), F32)
    for k in range(chunks):
        dl_loads[k].wait()
        latent += dot(tokens[:, k * step : (k + 1) * step], dl[k * step : (k + 1) * step, :])
    dr_load.wait()
    turned = dot_nt(tokens[...], dr[...])
    turned = jnp.concatenate([turned, jnp.zeros((rows, LANES - ROPE), F32)], axis=1)
    own_rows = pl.ds(pl.multiple_of(tp * rows, rows), rows)
    mine = block_rows(block(o, i, g, c))
    kv[mine, :rank] = normed(latent, lg_ref[...]).astype(BF16)
    kv[mine, rank:] = turn(turned, cos_ref[own_rows, :], sin_ref[own_rows, :]).astype(BF16)

    pl.semaphore_wait(barrier, O - 1 + 3)

    def up_copy(d):
        return kv_copy(block(o, i, g, c), dev((o + d) % O, i, g, c), d)

    def relay_near(d, act):
        b = block(o - d, i, g, c)
        act(kv_copy(b, across, O + d))

        @pl.when((i == 0) | (d > 0))
        def _():
            act(kv_copy(b, beside, 2 * O + 2 * d))

        act(kv_copy(b, mate, 4 * O + 4 * d))

    def relay_far(d, act):
        b = block(o - d, i, 1 - g, c)

        @pl.when(((i == 0) | (d > 0)) & (d < O - 1))
        def _():
            act(kv_copy(b, beside, 2 * O + 2 * d + 1))

        act(kv_copy(b, mate, 4 * O + 4 * d + 1))

    def relay_beside(d, act):
        b = block(o - d, 1 - i, g, c)

        @pl.when(d == O - 1)
        def _():
            act(kv_copy(b, across, 2 * O + 2 * d + 1))

        act(kv_copy(b, mate, 4 * O + 4 * d + 2))

    def relay_corner(d, act):
        act(kv_copy(block(o - d, 1 - i, 1 - g, c), mate, 4 * O + 4 * d + 3))

    def start(copy):
        copy.start()

    def sent(copy):
        copy.wait_send()

    def near(d):
        kv_wait(block(o - d, i, g, c))
        relay_near(d, start)

    def far(d):
        kv_wait(block(o - d, i, 1 - g, c))
        relay_far(d, start)

    def beside_in(d):
        kv_wait(block(o - d, 1 - i, g, c))
        relay_beside(d, start)

    def corner_in(d):
        kv_wait(block(o - d, 1 - i, 1 - g, c))
        relay_corner(d, start)

    def each(first, body):
        def run(d, carry):
            body(d)
            return carry

        lax.fori_loop(first, o + 1, run, 0)

    for d in range(1, O):

        @pl.when(o + d < O)
        def _(d=d):
            up_copy(d).start()

    relay_near(0, start)

    query = jnp.zeros((rows, dq.shape[1]), F32)
    for k in range(chunks):
        dq_loads[k].wait()
        query += dot(tokens[:, k * step : (k + 1) * step], dq[k * step : (k + 1) * step, :])
    ql[own_rows, :] = normed(query, qg_ref[...]).astype(BF16)

    def q_copy(t, target, index):
        part = ql.at[block_rows(t)]
        return pltpu.make_async_remote_copy(
            src_ref=part,
            dst_ref=part,
            send_sem=q_send.at[index],
            recv_sem=q_recv.at[t],
            device_id=target,
            device_id_type=MESH,
        )

    other = (1 - g) * 2 + c
    q_copies = [q_copy(tp, across, 0), q_copy(tp, mate, 1), q_copy(other, mate, 2)]
    q_copies[0].start()
    q_copies[1].start()

    def kv_heads(s):
        part = pl.ds(pl.multiple_of(s * span, span), span)
        lat = kv[part, :rank]
        return dot(lat, uk[...]).astype(BF16), dot_nt(uvt[...], lat).astype(BF16)

    up_loads[2].wait()
    up_loads[3].wait()
    uvt[...] = uv[...].T
    far(0)
    pl.when(o >= 1)(lambda: near(1))
    kv_wait(block(o, i, g, 1 - c))
    kv_wait(block(o, i, 1 - g, 1 - c))
    first_keys[...], first_values[...] = kv_heads(sp)
    each(2, near)

    q_copy(other, mate, 2).wait_recv()
    q_copies[2].start()

    @pl.when(i == 1)
    def _():
        beside_in(0)
        corner_in(0)

    q_copy(g * 2 + 1 - c, mate, 0).wait_recv()
    q_copy((1 - g) * 2 + 1 - c, mate, 0).wait_recv()

    pl.when(o >= 1)(lambda: far(1))
    for copy in up_loads[:2]:
        copy.wait()
    scale = (NOPE + ROPE) ** (-0.5) * log2e
    plain = (dot(ql[...], uq[...]) * scale).astype(BF16)
    turning = dot(ql[...], ur[...]) * scale
    low = lax.broadcasted_iota(jnp.int32, (span, LANES), 1) < ROPE
    for pair in range(heads // 2):
        both = turn(turning[:, pair * LANES : (pair + 1) * LANES], cos_ref[...], sin_ref[...])
        qh[2 * pair, :, NOPE:] = jnp.where(low, both, 0.0).astype(BF16)
        qh[2 * pair + 1, :, NOPE:] = jnp.where(low, pltpu.roll(both, ROPE, 1), 0.0).astype(BF16)
    for h in range(heads):
        qh[h, :, :NOPE] = plain[:, h * NOPE : (h + 1) * NOPE]
        best[h] = jnp.full(best.shape[1:], masked_score, F32)
        acc[h] = jnp.zeros(acc.shape[1:], F32)

    def attend(s, masked=False):
        rot = kv[pl.ds(pl.multiple_of(s * span, span), span), rank:]
        keys, values = (first_keys[...], first_values[...]) if masked else kv_heads(s)
        ones = jnp.ones((acc.shape[1] - VDIM, span), BF16)
        if masked:
            k_pos = lax.broadcasted_iota(jnp.int32, (span, span), 0)
            q_pos = lax.broadcasted_iota(jnp.int32, (span, span), 1)
            allowed = k_pos <= q_pos

        def score(h):
            key = jnp.concatenate([keys[:, h * NOPE : (h + 1) * NOPE], rot], axis=1)
            return dot_nt(key, qh[h])

        ahead = score(0)
        for h in range(heads):
            scores = ahead
            if h + 1 < heads:
                ahead = score(h + 1)
            value = jnp.concatenate([values[h * VDIM : (h + 1) * VDIM], ones], axis=0)
            if masked:
                scores = jnp.where(allowed, scores, masked_score)
            old = best[h][:1]
            new = jnp.maximum(old, jnp.max(scores, axis=0, keepdims=True))
            weights = jnp.exp2(scores - new).astype(BF16)
            acc[h] = acc[h] * jnp.exp2(old - new) + dot(value, weights)
            best[h] = jnp.broadcast_to(new, best.shape[1:])

    def next_to(d):
        kv_wait(block(o - d, 1 - i, g, 1 - c))
        kv_wait(block(o - d, 1 - i, 1 - g, 1 - c))
        attend((o - d) * 2 + 1 - i)

    def column(d):
        pl.when(d + 3 <= o)(lambda: far(d + 3))
        kv_wait(block(o - d, i, g, 1 - c))
        kv_wait(block(o - d, i, 1 - g, 1 - c))
        attend((o - d) * 2 + i)
        corner_in(d)

    attend(sp, masked=True)
    pl.when(o >= 2)(lambda: far(2))
    pl.when(i == 1)(lambda: next_to(0))
    pl.when(o >= 3)(lambda: far(3))
    each(1, beside_in)
    each(1, column)
    each(1, next_to)

    for h in range(heads):
        whole = acc[h]
        att[:, h * VDIM : (h + 1) * VDIM] = (whole[:VDIM] / whole[VDIM : VDIM + 1]).T.astype(BF16)

    ow_load.wait()
    width = ow.shape[1] // pieces
    lag = min(3, pieces)

    def pair_copy(phase, j):
        return pltpu.make_async_remote_copy(
            src_ref=pair_out.at[phase, j],
            dst_ref=pair_in.at[phase, j],
            send_sem=pair_send.at[phase * pieces + j],
            recv_sem=pair_recv.at[phase * pieces + j],
            device_id=mate,
            device_id_type=MESH,
        )

    def cross_copy(j):
        return pltpu.make_async_remote_copy(
            src_ref=cross_out.at[j],
            dst_ref=cross_in.at[j],
            send_sem=cross_send.at[j],
            recv_sem=cross_recv.at[j],
            device_id=across,
            device_id_type=MESH,
        )

    def project(phase, group, j):
        top = att[block_rows(group * 2 + 1 - c), :]
        low_part = att[block_rows(group * 2 + c), :]
        part = dot(jnp.concatenate([top, low_part], axis=0), ow[:, j * width : (j + 1) * width])
        pair_out[phase, j] = part[:rows].astype(BF16)
        kept[phase, j] = part[rows:]
        pair_copy(phase, j).start()

    def cross(j):
        pair_copy(0, j).wait_recv()
        cross_out[j] = (kept[0, j] + pair_in[0, j].astype(F32)).astype(BF16)
        cross_copy(j).start()

    for j in range(pieces):
        project(0, 1 - g, j)
        if j >= lag:
            cross(j - lag)
    for j in range(pieces - lag, pieces):
        cross(j)
    for j in range(pieces):
        project(1, g, j)
    for j in range(pieces):
        pair_copy(1, j).wait_recv()
        cross_copy(j).wait_recv()
        total = kept[1, j] + pair_in[1, j].astype(F32) + cross_in[j].astype(F32)
        out_ref[:, j * width : (j + 1) * width] = total

    for d in range(1, O):

        @pl.when(o + d < O)
        def _(d=d):
            up_copy(d).wait_send()

    def drain(d, carry):
        relay_near(d, sent)
        relay_far(d, sent)

        @pl.when((i == 1) | (d > 0))
        def _():
            relay_beside(d, sent)
            relay_corner(d, sent)

        return carry

    lax.fori_loop(0, o + 1, drain, 0)
    for copy in q_copies:
        copy.wait_send()
    for j in range(pieces):
        pair_copy(0, j).wait_send()
        pair_copy(1, j).wait_send()
        cross_copy(j).wait_send()


def solution(mesh):
    S, T = mesh.shape["sp"], mesh.shape["tp"]
    assert S % 2 == 0 and T == 4

    def local(tokens, dq, dl, dr, qg, lg, uq, ur, uk, uv, ow):
        rows, depth = tokens.shape
        span = rows * T
        heads = uk.shape[1] // NOPE
        width = ow.shape[1]
        rank = dl.shape[1]
        chunks, pieces = 4, 8
        inverse = np.float32(rope_base) ** (-np.arange(0, ROPE, 2, dtype=np.float32) / np.float32(ROPE))
        inverse = np.tile(inverse.astype(np.float64), LANES // (ROPE // 2))
        starts = np.arange(S)[:, None] * span * inverse
        steps = np.arange(span)[:, None] * inverse
        tables = [jnp.asarray(f(a), F32) for a in (starts, steps) for f in (np.cos, np.sin)]
        O = S // 2
        hbm = pl.BlockSpec(memory_space=pl.ANY)
        vmem = pl.BlockSpec(memory_space=pltpu.VMEM)
        dma = lambda n: pltpu.SemaphoreType.DMA((n,))
        like = lambda a: pltpu.VMEM(a.shape, a.dtype)
        total = pl.pallas_call(
            functools.partial(kernel, S, T, chunks, pieces),
            out_shape=jax.ShapeDtypeStruct((rows, width), F32),
            in_specs=[hbm, hbm, hbm, hbm, vmem, vmem, hbm, hbm, hbm, hbm, hbm, vmem, vmem, vmem, vmem],
            out_specs=vmem,
            scratch_shapes=[
                like(tokens),
                like(dq),
                like(dl),
                pltpu.VMEM(dr.shape[::-1], dr.dtype),
                like(uq),
                like(ur),
                like(uk),
                like(uv),
                like(ow),
                pltpu.VMEM((S * span, rank + LANES), BF16),
                pltpu.VMEM((span, dq.shape[1]), BF16),
                pltpu.VMEM((heads, span, NOPE + LANES), BF16),
                pltpu.VMEM((heads, VDIM + 16, span), F32),
                pltpu.VMEM((heads, 8, span), F32),
                pltpu.VMEM((span, heads * VDIM), BF16),
                pltpu.VMEM((2, pieces, rows, width // pieces), BF16),
                pltpu.VMEM((2, pieces, rows, width // pieces), BF16),
                pltpu.VMEM((2, pieces, rows, width // pieces), F32),
                pltpu.VMEM((pieces, rows, width // pieces), BF16),
                pltpu.VMEM((pieces, rows, width // pieces), BF16),
                pltpu.VMEM(uv.shape[::-1], BF16),
                pltpu.VMEM((span, heads * NOPE), BF16),
                pltpu.VMEM((heads * VDIM, span), BF16),
                pltpu.VMEM((span, LANES), F32),
                pltpu.VMEM((span, LANES), F32),
                dma(2 * chunks + 7),
                dma(8 * O),
                dma(S * T),
                dma(3),
                dma(T),
                dma(2 * pieces),
                dma(2 * pieces),
                dma(pieces),
                dma(pieces),
            ],
            compiler_params=pltpu.CompilerParams(
                collective_id=0, has_side_effects=True, vmem_limit_bytes=60 * 1024 * 1024
            ),
        )(
            tokens, dq, dl, dr.T, qg.reshape(1, -1), lg.reshape(1, -1),
            uq, ur, uk, uv, ow, *tables,
        )
        return total.astype(BF16)

    return jax.shard_map(
        local,
        mesh=mesh,
        in_specs=(
            P(("sp", "tp"), None),
            P(),
            P(),
            P(),
            P(),
            P(),
            P(None, "tp"),
            P(None, "tp"),
            P(None, "tp"),
            P(None, "tp"),
            P("tp", None),
        ),
        out_specs=P(("sp", "tp"), None),
        check_vma=False,
    )
```

profile of v0, /device:TPU:24, one launch (start us, length us, event | category | flops | bytes accessed | tf_op | source)
XLA Modules:
  0.0 45.0 jit_solution(7947134654214964572)
XLA Ops:
  0.0 42.9 %shard_map.145 = f32[64,4096]{1,0:T(8,128)} custom-call(bf16[64,4096]{1,0:T(8,128)(2,1)} %tokens_hbm.1, bf16[4096,1024]{1,0:T(8,128)(2,1)} %dq_hbm.1, bf16[4096,512]{1,0:T(8,128)(2,1)} %dl_hbm.1, bf16[64,4096]{1,0:T(8,128)(2,1)} %bitcast.3, f32[1,1024]{1,0:T(1,128)} %bitcast.4, f32[1,512]{1,0:T(1,128)} %bitcast.5, bf16[1024,512]{1,0:T(8,128)(2,1)} %uq_hbm.1, ...), custom_call_target="tpu_custom_call" | custom-call | tf_op jit(solution)/shard_map/pallas_call | solution.py:464
  42.9 2.1 %convert_element_type.3 = bf16[64,4096]{1,0:T(8,128)(2,1)} convert(f32[64,4096]{1,0:T(8,128)} %shard_map.145) | non-fusion elementwise | flops 262144 | bytes 1572864 | tf_op jit(solution)/shard_map/convert_element_type | solution.py:512
where the time goes:
time: 45.3 us; the launch traced here: 45 us
  Pallas kernels  42.9 us (95%)
  other arithmetic  2.07 us (5%)
    pallas_call x1, Pallas kernels, local(): pl.pallas_call(functools.partial(kernel, S, T, chunks, pieces), out_shape...  42.9 us
    convert_element_type x1, other arithmetic, local(): return total.astype(BF16)  2.07 us

commit v1 on v0

v1 whole, which is shorter than its diff:
```python
import functools

import jax
import jax.numpy as jnp
import numpy as np
from jax import lax
from jax.experimental import pallas as pl
from jax.experimental.pallas import tpu as pltpu
from jax.sharding import PartitionSpec as P

NOPE = 128
ROPE = 64
HALF = ROPE // 2
VDIM = 128
LANES = 128

rope_base = 500000.0
norm_eps = 1e-06
masked_score = -1e30
log2e = 1.4426950408889634

MESH = pl.DeviceIdType.MESH
F32 = jnp.float32
BF16 = jnp.bfloat16


def dot(a, b):
    return jnp.dot(a, b, preferred_element_type=F32)


def dot_nt(a, b):
    return lax.dot_general(a, b, (((1,), (1,)), ((), ())), preferred_element_type=F32)


def normed(v, gain):
    return v * lax.rsqrt(jnp.mean(v * v, axis=-1, keepdims=True) + norm_eps) * gain


def kernel(
    S,
    T,
    chunks,
    pieces,
    tokens_hbm,
    dq_hbm,
    dl_hbm,
    dr_hbm,
    qg_hbm,
    lg_hbm,
    uq_hbm,
    ur_hbm,
    uk_hbm,
    uv_hbm,
    ow_hbm,
    kbase_hbm,
    kstep_hbm,
    qbase_hbm,
    qstep_hbm,
    out_ref,
    tokens,
    dq,
    dl,
    dr,
    qg,
    lg,
    uq,
    ur,
    uk,
    uv,
    ow,
    kbase,
    kstep,
    qbase,
    qstep,
    kv,
    ql,
    qt,
    acc,
    best,
    att,
    pair_out,
    pair_in,
    kept,
    cross_out,
    cross_in,
    uqt,
    urt,
    uvt,
    keys,
    vals,
    rots,
    load_sem,
    kv_send,
    kv_recv,
    q_send,
    q_recv,
    pair_send,
    pair_recv,
    cross_send,
    cross_recv,
):
    O = S // 2
    rows = tokens.shape[0]
    span = rows * T
    depth = tokens.shape[1]
    heads = qt.shape[0]
    rank = dl.shape[1]
    slabs = rank // LANES
    sp = lax.axis_index("sp")
    tp = lax.axis_index("tp")
    o, i = sp // 2, sp % 2
    g, c = tp // 2, tp % 2

    def dev(o_, i_, g_, c_):
        return {"sp": o_ * 2 + i_, "tp": g_ * 2 + c_}

    across = dev(o, i, 1 - g, c)
    beside = dev(o, 1 - i, g, c)
    mate = dev(o, i, g, 1 - c)

    barrier = pltpu.get_barrier_semaphore()
    for d in range(1, O):
        pl.semaphore_signal(barrier, inc=1, device_id=dev((o + d) % O, i, g, c), device_id_type=MESH)
    for target in (across, beside, mate):
        pl.semaphore_signal(barrier, inc=1, device_id=target, device_id_type=MESH)

    step = depth // chunks
    loads = []

    def load(src, dst):
        copy = pltpu.make_async_copy(src, dst, load_sem.at[len(loads)])
        loads.append(copy)
        copy.start()
        return copy

    tok_load = load(tokens_hbm, tokens)
    dr_load = load(dr_hbm, dr)
    dl_loads = [load(dl_hbm.at[pl.ds(k * step, step)], dl.at[pl.ds(k * step, step)]) for k in range(chunks)]
    key_loads = [load(lg_hbm, lg), load(kbase_hbm.at[sp * T + tp], kbase), load(kstep_hbm, kstep)]
    dq_loads = [load(dq_hbm.at[pl.ds(k * step, step)], dq.at[pl.ds(k * step, step)]) for k in range(chunks)]
    qg_load = load(qg_hbm, qg)
    up_loads = [load(uv_hbm, uv), load(uq_hbm, uq), load(ur_hbm, ur)]
    uk_load = load(uk_hbm, uk)
    table_loads = [load(qbase_hbm.at[sp], qbase), load(qstep_hbm, qstep)]
    ow_load = load(ow_hbm, ow)

    def block(o_, i_, g_, c_):
        return (o_ * 2 + i_) * T + g_ * 2 + c_

    def block_rows(b):
        return pl.ds(pl.multiple_of(b * rows, rows), rows)

    def kv_copy(b, target, index):
        part = kv.at[b]
        return pltpu.make_async_remote_copy(
            src_ref=part,
            dst_ref=part,
            send_sem=kv_send.at[index],
            recv_sem=kv_recv.at[b],
            device_id=target,
            device_id_type=MESH,
        )

    def kv_wait(b):
        kv_copy(b, mate, 0).wait_recv()

    lane = lax.broadcasted_iota(jnp.int32, (rows, LANES), 1)

    tok_load.wait()
    dr_load.wait()
    turned = dot_nt(tokens[...], dr[...])
    latent = jnp.zeros((rows, rank), F32)
    for k in range(chunks):
        dl_loads[k].wait()
        latent += dot(tokens[:, k * step : (k + 1) * step], dl[k * step : (k + 1) * step, :])
    for copy in key_loads:
        copy.wait()
    start_cos, start_sin = kbase[0:1, :], kbase[8:9, :]
    cosine = start_cos * kstep[:rows, :] - start_sin * kstep[rows:, :]
    sine = start_sin * kstep[:rows, :] + start_cos * kstep[rows:, :]
    turned = jnp.concatenate([turned, jnp.zeros((rows, LANES - ROPE), F32)], axis=1)
    low = lane % ROPE < HALF
    swapped = jnp.where(low, -pltpu.roll(turned, LANES - HALF, 1), pltpu.roll(turned, HALF, 1))
    turned = turned * cosine + swapped * sine
    packed = jnp.where(lane[: rows // 2] < ROPE, turned[: rows // 2], pltpu.roll(turned[rows // 2 :], ROPE, 1))
    mine = block(o, i, g, c)
    latent = normed(latent, lg[...]).astype(BF16)
    for k in range(slabs):
        kv[mine, k * rows : (k + 1) * rows, :] = latent[:, k * LANES : (k + 1) * LANES]
    kv[mine, slabs * rows :, :] = packed.astype(BF16)

    pl.semaphore_wait(barrier, O - 1 + 3)

    def start(copy):
        copy.start()

    def sent(copy):
        copy.wait_send()

    def up(b, first, act):
        for d in reversed(range(1, O)):

            @pl.when(o + d < O)
            def _(d=d):
                act(kv_copy(b, dev((o + d) % O, i, g, c), first + d))

    def relay_column(d, act):
        b = block(o - d, i, g, c)
        act(kv_copy(b, across, O + d))

        @pl.when((i == 0) | (d > 0))
        def _():
            act(kv_copy(b, beside, 2 * O + d))

        act(kv_copy(b, mate, 4 * O + 4 * d))

    def relay_across(d, act):
        b = block(o - d, i, 1 - g, c)

        @pl.when((d == 0) & ((i == 0) | (o < O - 1)))
        def _():
            act(kv_copy(b, beside, 0))

        act(kv_copy(b, mate, 4 * O + 4 * d + 1))

    def relay_beside(d, act):
        act(kv_copy(block(o - d, 1 - i, g, c), mate, 4 * O + 4 * d + 2))

    def relay_corner(d, act):
        b = block(o - d, 1 - i, 1 - g, c)

        @pl.when((i == 1) | (d > 0))
        def _():
            act(kv_copy(b, mate, 4 * O + 4 * d + 3))

    def column_in(d):
        kv_wait(block(o - d, i, g, c))
        relay_column(d, start)

    def across_in(d):
        kv_wait(block(o - d, i, 1 - g, c))
        relay_across(d, start)

    def beside_in(d):
        kv_wait(block(o - d, 1 - i, g, c))
        relay_beside(d, start)

    def corner_in(d):
        kv_wait(block(o - d, 1 - i, 1 - g, c))
        relay_corner(d, start)

    def each(first, last, body):
        def run(d, carry):
            body(d)
            return carry

        lax.fori_loop(first, last, run, 0)

    up(mine, 0, start)
    relay_column(0, start)

    query = jnp.zeros((rows, dq.shape[1]), F32)
    for k in range(chunks):
        dq_loads[k].wait()
        query += dot(tokens[:, k * step : (k + 1) * step], dq[k * step : (k + 1) * step, :])
    qg_load.wait()
    own_rows = pl.ds(pl.multiple_of(tp * rows, rows), rows)
    ql[own_rows, :] = normed(query, qg[...]).astype(BF16)

    def q_copy(t, target, index):
        part = ql.at[block_rows(t)]
        return pltpu.make_async_remote_copy(
            src_ref=part,
            dst_ref=part,
            send_sem=q_send.at[index],
            recv_sem=q_recv.at[t],
            device_id=target,
            device_id_type=MESH,
        )

    other = (1 - g) * 2 + c
    q_copies = [q_copy(tp, across, 0), q_copy(tp, mate, 1), q_copy(other, mate, 2)]
    q_copies[0].start()
    q_copies[1].start()

    for copy in up_loads:
        copy.wait()
    uk_load.wait()
    uvt[...] = uv[...].T

    def latents(s):
        return jnp.concatenate(
            [
                jnp.concatenate([kv[s * T + t, k * rows : (k + 1) * rows, :] for k in range(slabs)], axis=1)
                for t in range(T)
            ],
            axis=0,
        )

    def rotaries(s):
        parts = []
        for t in range(T):
            both = kv[s * T + t, slabs * rows :, :].astype(F32)
            parts += [both, pltpu.roll(both, ROPE, 1)]
        return jnp.concatenate(parts, axis=0).astype(BF16)

    wide = 2 * LANES

    def head_parts(s, slot):
        lat = latents(s)

        def key_part(n):
            keys[slot, :, n : n + wide] = dot(lat, uk[:, n : n + wide]).astype(BF16)

        def value_part(n):
            vals[slot, n : n + wide, :] = dot_nt(uvt[n : n + wide, :], lat).astype(BF16)

        def rotary_part():
            rots[slot] = rotaries(s)

        parts = [functools.partial(key_part, n) for n in range(0, heads * NOPE, wide)]
        parts += [functools.partial(value_part, n) for n in range(0, heads * VDIM, wide)]
        return [rotary_part] + parts

    def kv_heads(s, slot):
        for part in head_parts(s, slot):
            part()

    across_in(0)
    pl.when(o >= 1)(lambda: column_in(1))
    pl.when(i == 1)(lambda: beside_in(0))
    uqt[...] = uq[...].T
    urt[...] = ur[...].T
    kv_wait(block(o, i, g, 1 - c))
    kv_wait(block(o, i, 1 - g, 1 - c))
    kv_heads(sp, 0)
    each(2, o + 1, column_in)

    @pl.when((i == 1) | (o < O - 1))
    def _():
        corner_in(0)
        up(block(o, 1 - i, 1 - g, c), 3 * O, start)

    q_copy(other, mate, 2).wait_recv()
    q_copies[2].start()
    for copy in table_loads:
        copy.wait()
    q_cos = jnp.concatenate([qbase[:HALF, :]] * (span // LANES), axis=1)
    q_sin = jnp.concatenate([qbase[HALF:, :]] * (span // LANES), axis=1)
    step_cos, step_sin = qstep[:HALF, :], qstep[HALF:, :]
    q_cos, q_sin = q_cos * step_cos - q_sin * step_sin, q_sin * step_cos + q_cos * step_sin
    q_copy(g * 2 + 1 - c, mate, 0).wait_recv()
    q_copy((1 - g) * 2 + 1 - c, mate, 0).wait_recv()

    scale = (NOPE + ROPE) ** (-0.5) * log2e
    plain = dot_nt(uqt[...], ql[...]) * scale
    turning = dot_nt(urt[...], ql[...]) * scale
    for h in range(heads):
        qt[h, :NOPE, :] = plain[h * NOPE : (h + 1) * NOPE, :].astype(BF16)
        first = turning[h * ROPE : h * ROPE + HALF, :]
        second = turning[h * ROPE + HALF : (h + 1) * ROPE, :]
        qt[h, NOPE : NOPE + HALF, :] = (first * q_cos - second * q_sin).astype(BF16)
        qt[h, NOPE + HALF : NOPE + ROPE, :] = (second * q_cos + first * q_sin).astype(BF16)
        qt[h, NOPE + ROPE :, :] = jnp.zeros((LANES - ROPE, span), BF16)

    def attend(slot, first=False, ahead=None):
        rot = rots[slot]
        ones = jnp.ones((acc.shape[1] - VDIM, span), BF16)
        parts = [] if ahead is None else head_parts(*ahead)
        if first:
            k_pos = lax.broadcasted_iota(jnp.int32, (span, span), 0)
            q_pos = lax.broadcasted_iota(jnp.int32, (span, span), 1)
            allowed = k_pos <= q_pos

        def score(h):
            key = jnp.concatenate([keys[slot, :, h * NOPE : (h + 1) * NOPE], rot], axis=1)
            return dot(key, qt[h])

        later = score(0)
        for h in range(heads):
            scores = later
            if h + 1 < heads:
                later = score(h + 1)
            for part in parts[h::heads]:
                part()
            value = jnp.concatenate([vals[slot, h * VDIM : (h + 1) * VDIM, :], ones], axis=0)
            if first:
                scores = jnp.where(allowed, scores, masked_score)
            new = jnp.max(scores, axis=0, keepdims=True)
            if not first:
                old = best[h][:1]
                new = jnp.maximum(old, new)
            weights = jnp.exp2(scores - new).astype(BF16)
            if first:
                acc[h] = dot(value, weights)
            else:
                acc[h] = acc[h] * jnp.exp2(old - new) + dot(value, weights)
            best[h] = jnp.broadcast_to(new, best.shape[1:])

    def relay_in(s):
        d, same = o - s // 2, s % 2 == i
        pl.when((d > 0) & same)(lambda: across_in(d))

        @pl.when((d > 0) & jnp.logical_not(same))
        def _():
            beside_in(d)
            corner_in(d)

    def mate_in(s):
        kv_wait(s * T + g * 2 + 1 - c)
        kv_wait(s * T + (1 - g) * 2 + 1 - c)

    attend(0, first=True)

    @pl.when(sp >= 1)
    def _():
        relay_in(sp - 1)
        pl.when(sp >= 2)(lambda: relay_in(sp - 2))
        mate_in(sp - 1)
        kv_heads(sp - 1, 1)

        def both(j):
            pl.when(sp - j >= 2)(lambda: relay_in(sp - j - 2))
            mate_in(sp - j - 1)
            attend(j % 2, ahead=(sp - j - 1, (j + 1) % 2))

        each(1, sp, both)
        attend(sp % 2)

    for h in range(heads):
        whole = acc[h]
        att[:, h * VDIM : (h + 1) * VDIM] = (whole[:VDIM] / whole[VDIM : VDIM + 1]).T.astype(BF16)

    ow_load.wait()
    width = ow.shape[1] // pieces
    lag = min(3, pieces)

    def pair_copy(phase, j):
        return pltpu.make_async_remote_copy(
            src_ref=pair_out.at[phase, j],
            dst_ref=pair_in.at[phase, j],
            send_sem=pair_send.at[phase * pieces + j],
            recv_sem=pair_recv.at[phase * pieces + j],
            device_id=mate,
            device_id_type=MESH,
        )

    def cross_copy(j):
        return pltpu.make_async_remote_copy(
            src_ref=cross_out.at[j],
            dst_ref=cross_in.at[j],
            send_sem=cross_send.at[j],
            recv_sem=cross_recv.at[j],
            device_id=across,
            device_id_type=MESH,
        )

    def project(phase, group, j):
        top = att[block_rows(group * 2 + 1 - c), :]
        low_part = att[block_rows(group * 2 + c), :]
        part = dot(jnp.concatenate([top, low_part], axis=0), ow[:, j * width : (j + 1) * width])
        pair_out[phase, j] = part[:rows].astype(BF16)
        kept[phase, j] = part[rows:]
        pair_copy(phase, j).start()

    def cross(j):
        pair_copy(0, j).wait_recv()
        cross_out[j] = (kept[0, j] + pair_in[0, j].astype(F32)).astype(BF16)
        cross_copy(j).start()

    for j in range(pieces):
        project(0, 1 - g, j)
        if j >= lag:
            cross(j - lag)
    for j in range(pieces - lag, pieces):
        cross(j)
    for j in range(pieces):
        project(1, g, j)

    up(mine, 0, sent)

    def drain(d):
        relay_column(d, sent)
        relay_across(d, sent)

        @pl.when((i == 1) | (d > 0))
        def _():
            relay_beside(d, sent)

        relay_corner(d, sent)

    each(0, o + 1, drain)
    pl.when((i == 1) | (o < O - 1))(lambda: up(block(o, 1 - i, 1 - g, c), 3 * O, sent))
    for copy in q_copies:
        copy.wait_send()

    for j in range(pieces):
        pair_copy(1, j).wait_recv()
        cross_copy(j).wait_recv()
        total = kept[1, j] + pair_in[1, j].astype(F32) + cross_in[j].astype(F32)
        out_ref[:, j * width : (j + 1) * width] = total.astype(BF16)

    for j in range(pieces):
        pair_copy(0, j).wait_send()
        pair_copy(1, j).wait_send()
        cross_copy(j).wait_send()


def solution(mesh):
    S, T = mesh.shape["sp"], mesh.shape["tp"]
    assert S % 2 == 0 and T == 4

    def local(tokens, dq, dl, dr, qg, lg, uq, ur, uk, uv, ow):
        rows, depth = tokens.shape
        span = rows * T
        heads = uk.shape[1] // NOPE
        width = ow.shape[1]
        rank = dl.shape[1]
        chunks, pieces = 4, 8
        inverse = np.float32(rope_base) ** (-np.arange(0, ROPE, 2, dtype=np.float32) / np.float32(ROPE))
        inverse = inverse.astype(np.float64)
        tiled = np.tile(inverse, LANES // HALF)

        def both(angles, axis):
            return np.concatenate([np.cos(angles), np.sin(angles)], axis=axis)

        key_base = np.repeat((np.arange(S * T) * rows)[:, None, None] * tiled, 8, axis=1)
        key_step = np.arange(rows)[:, None] * tiled
        query_base = np.repeat((np.arange(S) * span)[:, None, None] * inverse[:, None], LANES, axis=2)
        query_step = inverse[:, None] * np.arange(span)
        tables = [
            jnp.asarray(a, F32) for a in (both(key_base, 1), both(key_step, 0), both(query_base, 1), both(query_step, 0))
        ]
        O = S // 2
        hbm = pl.BlockSpec(memory_space=pl.ANY)
        vmem = pl.BlockSpec(memory_space=pltpu.VMEM)
        dma = lambda n: pltpu.SemaphoreType.DMA((n,))
        like = lambda a: pltpu.VMEM(a.shape, a.dtype)
        operands = [tokens, dq, dl, dr.T, qg.reshape(1, -1), lg.reshape(1, -1), uq, ur, uk, uv, ow, *tables]
        operands = [pltpu.with_memory_space_constraint(a, pltpu.HBM) for a in operands]
        block_height = rows * rank // LANES + rows // 2
        return pl.pallas_call(
            functools.partial(kernel, S, T, chunks, pieces),
            out_shape=jax.ShapeDtypeStruct((rows, width), BF16),
            in_specs=[hbm] * len(operands),
            out_specs=vmem,
            scratch_shapes=[
                *[like(a) for a in operands[:11]],
                pltpu.VMEM((16, LANES), F32),
                pltpu.VMEM((2 * rows, LANES), F32),
                pltpu.VMEM((ROPE, LANES), F32),
                pltpu.VMEM((ROPE, span), F32),
                pltpu.VMEM((S * T, block_height, LANES), BF16),
                pltpu.VMEM((span, dq.shape[1]), BF16),
                pltpu.VMEM((heads, NOPE + LANES, span), BF16),
                pltpu.VMEM((heads, VDIM + 16, span), F32),
                pltpu.VMEM((heads, 8, span), F32),
                pltpu.VMEM((span, heads * VDIM), BF16),
                pltpu.VMEM((2, pieces, rows, width // pieces), BF16),
                pltpu.VMEM((2, pieces, rows, width // pieces), BF16),
                pltpu.VMEM((2, pieces, rows, width // pieces), F32),
                pltpu.VMEM((pieces, rows, width // pieces), BF16),
                pltpu.VMEM((pieces, rows, width // pieces), BF16),
                pltpu.VMEM(uq.shape[::-1], BF16),
                pltpu.VMEM(ur.shape[::-1], BF16),
                pltpu.VMEM(uv.shape[::-1], BF16),
                pltpu.VMEM((2, span, heads * NOPE), BF16),
                pltpu.VMEM((2, heads * VDIM, span), BF16),
                pltpu.VMEM((2, span, LANES), BF16),
                dma(2 * chunks + 13),
                dma(8 * O),
                dma(S * T),
                dma(3),
                dma(T),
                dma(2 * pieces),
                dma(2 * pieces),
                dma(pieces),
                dma(pieces),
            ],
            compiler_params=pltpu.CompilerParams(
                collective_id=0, has_side_effects=True, vmem_limit_bytes=54 * 1024 * 1024
            ),
        )(*operands)

    return jax.shard_map(
        local,
        mesh=mesh,
        in_specs=(
            P(("sp", "tp"), None),
            P(),
            P(),
            P(),
            P(),
            P(),
            P(None, "tp"),
            P(None, "tp"),
            P(None, "tp"),
            P(None, "tp"),
            P("tp", None),
        ),
        out_specs=P(("sp", "tp"), None),
        check_vma=False,
    )
```

time: 45.3 us -> 43.5 us (0.960)
  other arithmetic: 2.07 us -> 0 us
  Pallas kernels: 42.9 us -> 40.9 us
  local copies, waits for them, and re-layouts: 0 us -> 1.87 us
    convert_element_type x1 -> x0, other arithmetic: 2.07 us -> none  [local(): return total.astype(BF16)]
    pallas_call x1, Pallas kernels: 42.9 us -> 40.9 us  [local(): pl.pallas_call(functools.partial(kernel, S, T, chunks, pieces), out_shape...]
    unnamed x0 -> x1, local copies, waits for them, and re-layouts: none -> 1.87 us
where the time goes in v1:
time: 43.5 us; the launch traced here: 42.8 us
  Pallas kernels  40.9 us (94%)
  local copies, waits for them, and re-layouts  1.87 us (4%)
    pallas_call x1, Pallas kernels, local(): pl.pallas_call(functools.partial(kernel, S, T, chunks, pieces), out_shape...  40.9 us
    unnamed x1, local copies, waits for them, and re-layouts  1.87 us

profile of v1, /device:TPU:24, one launch (start us, length us, event | category | flops | bytes accessed | tf_op | source)
XLA Modules:
  0.0 42.8 jit_solution(13325849144008449598)
XLA Ops:
  0.0 40.9 %shard_map.145 = bf16[64,4096]{1,0:T(8,128)(2,1)} custom-call(bf16[64,4096]{1,0:T(8,128)(2,1)} %tokens_hbm.1, bf16[4096,1024]{1,0:T(8,128)(2,1)} %dq_hbm.1, bf16[4096,512]{1,0:T(8,128)(2,1)} %dl_hbm.1, bf16[64,4096]{1,0:T(8,128)(2,1)} %bitcast.3, f32[1,1024]{1,0:T(1,128)} %bitcast.4, f32[1,512]{1,0:T(1,128)} %bitcast.5, bf16[1024,512]{1,0:T(8,128)(2,1)} %uq_hbm.1, ...), custom_call_target="tpu_custom_call" | custom-call | tf_op jit(solution)/shard_map/pallas_call | solution.py:542
  41.0 1.9 %copy.17 = bf16[64,4096]{1,0:T(8,128)(2,1)} copy(bf16[64,4096]{1,0:T(8,128)(2,1)} %shard_map.145) | data formatting | bytes 1048576

commit v2 on v1

v2 whole, which is shorter than its diff:
```python
import functools

import jax
import jax.numpy as jnp
import numpy as np
from jax import lax
from jax.experimental import pallas as pl
from jax.experimental.pallas import tpu as pltpu
from jax.sharding import PartitionSpec as P

NOPE = 128
ROPE = 64
HALF = ROPE // 2
VDIM = 128
LANES = 128

rope_base = 500000.0
norm_eps = 1e-06
masked_score = -1e30
log2e = 1.4426950408889634

MESH = pl.DeviceIdType.MESH
F32 = jnp.float32
BF16 = jnp.bfloat16


def dot(a, b):
    return jnp.dot(a, b, preferred_element_type=F32)


def dot_nt(a, b):
    return lax.dot_general(a, b, (((1,), (1,)), ((), ())), preferred_element_type=F32)


def normed(v, gain):
    return v * lax.rsqrt(jnp.mean(v * v, axis=-1, keepdims=True) + norm_eps) * gain


def kernel(
    S,
    T,
    chunks,
    pieces,
    tokens_hbm,
    dq_hbm,
    dl_hbm,
    dr_hbm,
    qg_hbm,
    lg_hbm,
    uq_hbm,
    ur_hbm,
    uk_hbm,
    uv_hbm,
    ow_hbm,
    kbase_hbm,
    kstep_hbm,
    qbase_hbm,
    qstep_hbm,
    out_ref,
    tokens,
    dq,
    dl,
    dr,
    qg,
    lg,
    uq,
    ur,
    uk,
    uv,
    ow,
    kbase,
    kstep,
    qbase,
    qstep,
    kv,
    ql,
    qt,
    acc,
    best,
    att,
    pair_out,
    pair_in,
    kept,
    cross_out,
    cross_in,
    uqt,
    urt,
    uvt,
    keys,
    vals,
    rots,
    scored,
    load_sem,
    kv_send,
    kv_recv,
    q_send,
    q_recv,
    pair_send,
    pair_recv,
    cross_send,
    cross_recv,
):
    O = S // 2
    rows = tokens.shape[0]
    span = rows * T
    depth = tokens.shape[1]
    heads = qt.shape[1]
    rank = dl.shape[1]
    slabs = rank // LANES
    sp = lax.axis_index("sp")
    tp = lax.axis_index("tp")
    o, i = sp // 2, sp % 2
    g, c = tp // 2, tp % 2

    def dev(o_, i_, g_, c_):
        return {"sp": o_ * 2 + i_, "tp": g_ * 2 + c_}

    across = dev(o, i, 1 - g, c)
    beside = dev(o, 1 - i, g, c)
    mate = dev(o, i, g, 1 - c)

    barrier = pltpu.get_barrier_semaphore()
    for d in range(1, O):
        pl.semaphore_signal(barrier, inc=1, device_id=dev((o + d) % O, i, g, c), device_id_type=MESH)
    for target in (across, beside, mate):
        pl.semaphore_signal(barrier, inc=1, device_id=target, device_id_type=MESH)

    step = depth // chunks
    loads = []

    def load(src, dst):
        copy = pltpu.make_async_copy(src, dst, load_sem.at[len(loads)])
        loads.append(copy)
        copy.start()
        return copy

    tok_load = load(tokens_hbm, tokens)
    dr_load = load(dr_hbm, dr)
    dl_loads = [load(dl_hbm.at[pl.ds(k * step, step)], dl.at[pl.ds(k * step, step)]) for k in range(chunks)]
    key_loads = [load(lg_hbm, lg), load(kbase_hbm.at[sp * T + tp], kbase), load(kstep_hbm, kstep)]
    dq_loads = [load(dq_hbm.at[pl.ds(k * step, step)], dq.at[pl.ds(k * step, step)]) for k in range(chunks)]
    qg_load = load(qg_hbm, qg)
    up_loads = [load(uv_hbm, uv), load(uq_hbm, uq), load(ur_hbm, ur)]
    uk_load = load(uk_hbm, uk)
    table_loads = [load(qbase_hbm.at[sp], qbase), load(qstep_hbm, qstep)]
    ow_load = load(ow_hbm, ow)

    def block(o_, i_, g_, c_):
        return (o_ * 2 + i_) * T + g_ * 2 + c_

    def block_rows(b):
        return pl.ds(pl.multiple_of(b * rows, rows), rows)

    def kv_copy(o_, i_, g_, target, index):
        s = o_ * 2 + i_
        part = kv.at[s * T + g_ * 2 + c]
        return pltpu.make_async_remote_copy(
            src_ref=part,
            dst_ref=part,
            send_sem=kv_send.at[index],
            recv_sem=kv_recv.at[2 * S + s if target is mate else 2 * s + g_],
            device_id=target,
            device_id_type=MESH,
        )

    def kv_wait(o_, i_, g_):
        kv_copy(o_, i_, g_, across, 0).wait_recv()

    def kv_blocks(count, send, receive):
        part = kv.at[pl.ds(0, count)]
        return pltpu.make_async_remote_copy(
            src_ref=part,
            dst_ref=part,
            send_sem=kv_send.at[send],
            recv_sem=kv_recv.at[receive],
            device_id=mate,
            device_id_type=MESH,
        )

    def mate_in(s):
        kv_blocks(2, 0, 2 * S + s).wait_recv()

    wide = 2 * LANES
    mine = block(o, i, g, c)

    side = span // 2

    def phase(body):
        pl.when(sp < S)(body)

    def projected(weight, weight_loads):
        sums = [jnp.zeros((rows, wide), F32) for _ in range(weight.shape[1] // wide)]
        for k in range(chunks):
            weight_loads[k].wait()
            part = tokens[:, k * step : (k + 1) * step]
            for n in range(len(sums)):
                sums[n] += dot(part, weight[k * step : (k + 1) * step, n * wide : (n + 1) * wide])
        return jnp.concatenate(sums, axis=1)

    @phase
    def _():
        tok_load.wait()
        dr_load.wait()
        turned = dot_nt(tokens[...], dr[...])
        latent = projected(dl, dl_loads)
        for copy in key_loads:
            copy.wait()
        lane = lax.broadcasted_iota(jnp.int32, (rows, LANES), 1)
        start_cos, start_sin = kbase[0:1, :], kbase[8:9, :]
        cosine = start_cos * kstep[:rows, :] - start_sin * kstep[rows:, :]
        sine = start_sin * kstep[:rows, :] + start_cos * kstep[rows:, :]
        turned = jnp.concatenate([turned, jnp.zeros((rows, LANES - ROPE), F32)], axis=1)
        low = lane % ROPE < HALF
        swapped = jnp.where(low, -pltpu.roll(turned, LANES - HALF, 1), pltpu.roll(turned, HALF, 1))
        turned = turned * cosine + swapped * sine
        packed = jnp.where(lane[: rows // 2] < ROPE, turned[: rows // 2], pltpu.roll(turned[rows // 2 :], ROPE, 1))
        latent = normed(latent, lg[...]).astype(BF16)
        for k in range(slabs):
            kv[mine, k * rows : (k + 1) * rows, :] = latent[:, k * LANES : (k + 1) * LANES]
        kv[mine, slabs * rows :, :] = packed.astype(BF16)

    pl.semaphore_wait(barrier, O - 1 + 3)

    def up(g_, i_):
        def send(d, allowed):
            @pl.when((o + d < O) & allowed)
            def _():
                kv_copy(o, i_, g_, dev((o + d) % O, i, g, c), O + d - 1).start()

        for d in reversed(range(1, O)):
            send(d, (o > 0) | (d == O - 1))
        for d in range(1, O - 1):
            send(d, (o == 0) & ((d != O - 2) | (O < 4) | (g_ is not g)))

    def relay_column(d):
        @pl.when((d == O - 1) & (O >= 4))
        def _():
            kv_copy(o - d, i, g, dev(O - 2, i, g, c), d).start()

        kv_copy(o - d, i, g, across, d).start()

        @pl.when((i == 0) | (d > 0))
        def _():
            kv_copy(o - d, i, g, beside, d).start()

        kv_copy(o - d, i, g, mate, d).start()

    def column_in(d):
        kv_wait(o - d, i, g)
        relay_column(d)

    def across_in(d):
        kv_wait(o - d, i, 1 - g)
        kv_copy(o - d, i, 1 - g, mate, d).start()

    def beside_in(d):
        kv_wait(o - d, 1 - i, g)
        kv_copy(o - d, 1 - i, g, mate, d).start()

    def corner_in(d):
        kv_wait(o - d, 1 - i, 1 - g)

        @pl.when((i == 1) | (d > 0))
        def _():
            kv_copy(o - d, 1 - i, 1 - g, mate, d).start()

    def each(first, last, body):
        def run(d, carry):
            body(d)
            return carry

        lax.fori_loop(first, last, run, 0)

    up(g, i)
    relay_column(0)

    own_rows = pl.ds(pl.multiple_of(tp * rows, rows), rows)

    @phase
    def _():
        query = projected(dq, dq_loads)
        qg_load.wait()
        ql[own_rows, :] = normed(query, qg[...]).astype(BF16)

    def q_copy(t, target):
        part = ql.at[block_rows(t)]
        return pltpu.make_async_remote_copy(
            src_ref=part,
            dst_ref=part,
            send_sem=q_send.at[0],
            recv_sem=q_recv.at[t],
            device_id=target,
            device_id_type=MESH,
        )

    other = (1 - g) * 2 + c
    q_copy(tp, across).start()
    q_copy(tp, mate).start()

    for copy in up_loads:
        copy.wait()
    uk_load.wait()
    uvt[...] = uv[...].T

    def latents(s):
        return jnp.concatenate(
            [
                jnp.concatenate([kv[s * T + t, k * rows : (k + 1) * rows, :] for k in range(slabs)], axis=1)
                for t in range(T)
            ],
            axis=0,
        )

    def rotaries(s):
        parts = []
        for t in range(T):
            both = kv[s * T + t, slabs * rows :, :].astype(F32)
            parts += [both, pltpu.roll(both, ROPE, 1)]
        return jnp.concatenate(parts, axis=0).astype(BF16)

    def head_parts(s, slot):
        lat = latents(s)

        def key_part(n):
            keys[slot, :, n : n + wide] = dot(lat, uk[:, n : n + wide]).astype(BF16)

        def value_part(n):
            vals[slot, n : n + wide, :] = dot_nt(uvt[n : n + wide, :], lat).astype(BF16)

        def rotary_part():
            rots[slot] = rotaries(s)

        parts = [functools.partial(key_part, n) for n in range(0, heads * NOPE, wide)]
        parts += [functools.partial(value_part, n) for n in range(0, heads * VDIM, wide)]
        return [rotary_part] + parts

    def kv_heads(s, slot):
        for part in head_parts(s, slot):
            part()

    def relay_in(s):
        d, same = o - s // 2, s % 2 == i
        pl.when((d > 0) & same)(lambda: across_in(d))

        @pl.when((d > 0) & jnp.logical_not(same))
        def _():
            beside_in(d)
            corner_in(d)

    across_in(0)

    @pl.when((i == 0) | (o < O - 1))
    def _():
        kv_copy(o, i, 1 - g, beside, 2 * O - 1).start()

    pl.when((o >= 1) & (o == O - 1))(lambda: column_in(1))
    pl.when(i == 1)(lambda: beside_in(0))
    uqt[...] = uq[...].T
    urt[...] = ur[...].T
    mate_in(sp)
    phase(lambda: kv_heads(sp, 0))

    @pl.when((i == 1) | (o < O - 1))
    def _():
        corner_in(0)
        up(1 - g, 1 - i)

    pl.when((o >= 1) & (o < O - 1))(lambda: column_in(1))

    pl.when(o == O - 1)(lambda: each(2, o + 1, column_in))
    q_copy(other, mate).wait_recv()
    q_copy(other, mate).start()

    def seq(j):
        return sp - j - jnp.where(i == 1, 0, 2 * (j % 2) - 1)

    @pl.when(i == 1)
    def _():
        mate_in(seq(1))
        kv_heads(seq(1), 1)

    pl.when((o >= 1) & (o == O - 1))(lambda: across_in(1))
    for copy in table_loads:
        copy.wait()
    q_cos = jnp.concatenate([qbase[:HALF, :]] * (span // LANES), axis=1)
    q_sin = jnp.concatenate([qbase[HALF:, :]] * (span // LANES), axis=1)
    step_cos, step_sin = qstep[:HALF, :], qstep[HALF:, :]
    q_cos, q_sin = q_cos * step_cos - q_sin * step_sin, q_sin * step_cos + q_cos * step_sin
    q_copy(g * 2 + 1 - c, mate).wait_recv()
    q_copy((1 - g) * 2 + 1 - c, mate).wait_recv()

    scale = (NOPE + ROPE) ** (-0.5) * log2e

    @phase
    def _():
        plain = dot_nt(uqt[...], ql[...]) * scale
        turning = dot_nt(urt[...], ql[...]) * scale
        for h in range(heads):
            first = turning[h * ROPE : h * ROPE + HALF, :]
            second = turning[h * ROPE + HALF : (h + 1) * ROPE, :]
            whole = [
                plain[h * NOPE : (h + 1) * NOPE, :],
                first * q_cos - second * q_sin,
                second * q_cos + first * q_sin,
                jnp.zeros((LANES - ROPE, span), F32),
            ]
            whole = jnp.concatenate(whole, axis=0).astype(BF16)
            for n in range(2):
                qt[n, h] = whole[:, n * side : (n + 1) * side]

    def score(slot, h, group):
        key = jnp.concatenate([keys[slot, :, h * NOPE : (h + 1) * NOPE], rots[slot]], axis=1)
        return dot(key, qt[group, h])

    def attend(slot, group, first=False, ahead=None):
        ones = jnp.ones((acc.shape[1] - VDIM, span), BF16)
        parts = [] if ahead is None else head_parts(*ahead)
        if first:
            k_pos = lax.broadcasted_iota(jnp.int32, (span, side), 0)
            q_pos = lax.broadcasted_iota(jnp.int32, (span, side), 1) + group * side
            allowed = k_pos <= q_pos
        later = score(slot, 0, group) if first else scored[...]
        for h in range(heads):
            scores = later
            if h + 1 < heads:
                later = score(slot, h + 1, group)
            for part in parts[h * len(parts) // heads : (h + 1) * len(parts) // heads]:
                part()
            value = jnp.concatenate([vals[slot, h * VDIM : (h + 1) * VDIM, :], ones], axis=0)
            if first:
                scores = jnp.where(allowed, scores, masked_score)
            new = jnp.max(scores, axis=0, keepdims=True)
            if not first:
                old = best[h][:1]
                new = jnp.maximum(old, new)
            weights = jnp.exp2(scores - new).astype(BF16)
            if first:
                acc[h] = dot(value, weights)
            else:
                acc[h] = acc[h] * jnp.exp2(old - new) + dot(value, weights)
            best[h] = jnp.broadcast_to(new, best.shape[1:])
        if ahead is not None:
            scored[...] = score(ahead[1], 0, group)

    def sweep(group, arriving):
        @pl.when(sp >= 1)
        def _():
            def both(j):
                if arriving:
                    pl.when((i == 0) & (j + 2 <= sp))(lambda: relay_in(seq(j + 2)))
                    mate_in(seq(j + 1))
                attend(j % 2, group, ahead=(seq(j + 1), (j + 1) % 2))
                if arriving:
                    pl.when((i == 1) & (j + 3 <= sp))(lambda: relay_in(seq(j + 3)))

            each(1, sp, both)
            attend(sp % 2, group)

        @phase
        def _():
            for h in range(heads):
                whole = acc[h]
                part = (whole[:VDIM] / whole[VDIM : VDIM + 1]).T.astype(BF16)
                att[pl.ds(pl.multiple_of(group * side, side), side), h * VDIM : (h + 1) * VDIM] = part

    phase(lambda: attend(0, 1 - g, first=True))

    @pl.when((o >= 1) & (o < O - 1))
    def _():
        each(2, o + 1, column_in)
        across_in(1)

    @pl.when(o >= 1)
    def _():
        beside_in(1)
        corner_in(1)

    @pl.when(sp >= 1)
    def _():
        @pl.when(i == 0)
        def _():
            mate_in(seq(1))
            kv_heads(seq(1), 1)

        phase(lambda: scored.__setitem__(..., score(1, 0, 1 - g)))

    sweep(1 - g, True)

    ow_load.wait()
    width = ow.shape[1] // pieces
    lag = min(3, pieces)

    def pair_copy(second, j):
        return pltpu.make_async_remote_copy(
            src_ref=pair_out.at[second, j],
            dst_ref=pair_in.at[second, j],
            send_sem=pair_send.at[0],
            recv_sem=pair_recv.at[pieces if second else j],
            device_id=mate,
            device_id_type=MESH,
        )

    def cross_copy(j):
        return pltpu.make_async_remote_copy(
            src_ref=cross_out.at[j],
            dst_ref=cross_in.at[j],
            send_sem=cross_send.at[0],
            recv_sem=cross_recv.at[j],
            device_id=across,
            device_id_type=MESH,
        )

    def project(second, group, j):
        top = att[block_rows(group * 2 + 1 - c), :]
        low_part = att[block_rows(group * 2 + c), :]
        part = dot(jnp.concatenate([top, low_part], axis=0), ow[:, j * width : (j + 1) * width])
        pair_out[second, j] = part[:rows].astype(BF16)
        kept[second, j] = part[rows:]
        pair_copy(second, j).start()

    def cross(j):
        pair_copy(0, j).wait_recv()
        cross_out[j] = (kept[0, j] + pair_in[0, j].astype(F32)).astype(BF16)
        cross_copy(j).start()

    @phase
    def _():
        for j in range(pieces):
            project(0, 1 - g, j)
            if j >= lag:
                cross(j - lag)
        for j in range(pieces - lag, pieces):
            cross(j)

    phase(lambda: kv_heads(sp, 0))
    phase(lambda: attend(0, g, first=True))

    @pl.when(sp >= 1)
    def _():
        kv_heads(seq(1), 1)
        scored[...] = score(1, 0, g)

    sweep(g, False)

    @phase
    def _():
        for j in range(pieces):
            project(1, g, j)

    def all_sent(n, copies):
        pltpu.make_async_remote_copy(
            src_ref=n, dst_ref=n, send_sem=copies.at[0], recv_sem=q_recv.at[0], device_id=mate, device_id_type=MESH
        ).wait_send()

    pl.when(i == 0)(lambda: kv_blocks(4, 0, 0).wait_send())
    pl.when(i == 1)(lambda: kv_blocks(5, 0, 0).wait_send())
    pl.when((i == 0) | (o < O - 1))(lambda: kv_blocks(1, 2 * O - 1, 0).wait_send())

    def some_sent(few, count, index):
        pl.when(few)(lambda: kv_blocks(count - 1, index, 0).wait_send())
        pl.when(jnp.logical_not(few))(lambda: kv_blocks(count, index, 0).wait_send())

    each(1, o + 1, lambda d: some_sent((d < O - 1) | (O < 4), 7, d))
    each(1, O - o, lambda d: some_sent((o == 0) & (d == O - 2) & (O >= 4), 2, O + d - 1))
    all_sent(ql.at[pl.ds(0, 3 * rows)], q_send)
    all_sent(pair_out, pair_send)
    pltpu.make_async_remote_copy(
        src_ref=pair_out.at[1],
        dst_ref=pair_in.at[1],
        send_sem=pair_send.at[0],
        recv_sem=pair_recv.at[pieces],
        device_id=mate,
        device_id_type=MESH,
    ).wait_recv()
    for j in range(pieces):
        cross_copy(j).wait_recv()
        total = kept[1, j] + pair_in[1, j].astype(F32) + cross_in[j].astype(F32)
        out_ref[:, j * width : (j + 1) * width] = total.astype(BF16)
    all_sent(cross_out, cross_send)


def solution(mesh):
    S, T = mesh.shape["sp"], mesh.shape["tp"]
    assert S % 2 == 0 and T == 4

    def local(tokens, dq, dl, dr, qg, lg, uq, ur, uk, uv, ow):
        rows, depth = tokens.shape
        span = rows * T
        heads = uk.shape[1] // NOPE
        width = ow.shape[1]
        rank = dl.shape[1]
        chunks, pieces = 4, 8
        inverse = np.float32(rope_base) ** (-np.arange(0, ROPE, 2, dtype=np.float32) / np.float32(ROPE))
        inverse = inverse.astype(np.float64)
        tiled = np.tile(inverse, LANES // HALF)

        def both(angles, axis):
            return np.concatenate([np.cos(angles), np.sin(angles)], axis=axis)

        key_base = np.repeat((np.arange(S * T) * rows)[:, None, None] * tiled, 8, axis=1)
        key_step = np.arange(rows)[:, None] * tiled
        query_base = np.repeat((np.arange(S) * span)[:, None, None] * inverse[:, None], LANES, axis=2)
        query_step = inverse[:, None] * np.arange(span)
        tables = [
            jnp.asarray(a, F32) for a in (both(key_base, 1), both(key_step, 0), both(query_base, 1), both(query_step, 0))
        ]
        O = S // 2
        hbm = pl.BlockSpec(memory_space=pl.ANY)
        vmem = pl.BlockSpec(memory_space=pltpu.VMEM)
        dma = lambda n: pltpu.SemaphoreType.DMA((n,))
        like = lambda a: pltpu.VMEM(a.shape, a.dtype)
        operands = [tokens, dq, dl, dr.T, qg.reshape(1, -1), lg.reshape(1, -1), uq, ur, uk, uv, ow, *tables]
        operands = [pltpu.with_memory_space_constraint(a, pltpu.HBM) for a in operands]
        block_height = rows * rank // LANES + rows // 2
        return pl.pallas_call(
            functools.partial(kernel, S, T, chunks, pieces),
            out_shape=jax.ShapeDtypeStruct((rows, width), BF16),
            in_specs=[hbm] * len(operands),
            out_specs=vmem,
            scratch_shapes=[
                *[like(a) for a in operands[:11]],
                pltpu.VMEM((16, LANES), F32),
                pltpu.VMEM((2 * rows, LANES), F32),
                pltpu.VMEM((ROPE, LANES), F32),
                pltpu.VMEM((ROPE, span), F32),
                pltpu.VMEM((S * T, block_height, LANES), BF16),
                pltpu.VMEM((span, dq.shape[1]), BF16),
                pltpu.VMEM((2, heads, NOPE + LANES, span // 2), BF16),
                pltpu.VMEM((heads, VDIM + 16, span // 2), F32),
                pltpu.VMEM((heads, 8, span // 2), F32),
                pltpu.VMEM((span, heads * VDIM), BF16),
                pltpu.VMEM((2, pieces, rows, width // pieces), BF16),
                pltpu.VMEM((2, pieces, rows, width // pieces), BF16),
                pltpu.VMEM((2, pieces, rows, width // pieces), F32),
                pltpu.VMEM((pieces, rows, width // pieces), BF16),
                pltpu.VMEM((pieces, rows, width // pieces), BF16),
                pltpu.VMEM(uq.shape[::-1], BF16),
                pltpu.VMEM(ur.shape[::-1], BF16),
                pltpu.VMEM(uv.shape[::-1], BF16),
                pltpu.VMEM((2, span, heads * NOPE), BF16),
                pltpu.VMEM((2, heads * VDIM, span), BF16),
                pltpu.VMEM((2, span, LANES), BF16),
                pltpu.VMEM((span, span // 2), F32),
                dma(2 * chunks + 13),
                dma(2 * O),
                dma(3 * S),
                dma(1),
                dma(T),
                dma(1),
                dma(pieces + 1),
                dma(1),
                dma(pieces),
            ],
            compiler_params=pltpu.CompilerParams(
                collective_id=0, has_side_effects=True, vmem_limit_bytes=46 * 1024 * 1024
            ),
        )(*operands)

    return jax.shard_map(
        local,
        mesh=mesh,
        in_specs=(
            P(("sp", "tp"), None),
            P(),
            P(),
            P(),
            P(),
            P(),
            P(None, "tp"),
            P(None, "tp"),
            P(None, "tp"),
            P(None, "tp"),
            P("tp", None),
        ),
        out_specs=P(("sp", "tp"), None),
        check_vma=False,
    )
```

time: 43.5 us -> 37.9 us (0.87)
  Pallas kernels: 40.9 us -> 36.6 us
  local copies, waits for them, and re-layouts: 1.87 us -> 0.8 us
    pallas_call x1, Pallas kernels: 40.9 us -> 36.6 us  [local(): pl.pallas_call(functools.partial(kernel, S, T, chunks, pieces), out_shape...]
    unnamed x1, local copies, waits for them, and re-layouts: 1.87 us -> 0.8 us
where the time goes in v2:
time: 37.9 us; the launch traced here: 37.4 us
  Pallas kernels  36.6 us (97%)
  local copies, waits for them, and re-layouts  0.8 us (2%)
    pallas_call x1, Pallas kernels, local(): pl.pallas_call(functools.partial(kernel, S, T, chunks, pieces), out_shape...  36.6 us
    unnamed x1, local copies, waits for them, and re-layouts  0.8 us

profile of v2, /device:TPU:24, one launch (start us, length us, event | category | flops | bytes accessed | tf_op | source)
XLA Modules:
  0.0 37.4 jit_solution(1410833333265771206)
XLA Ops:
  0.0 36.6 %shard_map.145 = bf16[64,4096]{1,0:T(8,128)(2,1)S(1)} custom-call(bf16[64,4096]{1,0:T(8,128)(2,1)} %tokens_hbm.1, bf16[4096,1024]{1,0:T(8,128)(2,1)} %dq_hbm.1, bf16[4096,512]{1,0:T(8,128)(2,1)} %dl_hbm.1, bf16[64,4096]{1,0:T(8,128)(2,1)} %bitcast.3, f32[1,1024]{1,0:T(1,128)} %bitcast.4, f32[1,512]{1,0:T(1,128)} %bitcast.5, bf16[1024,512]{1,0:T(8,128)(2,1)} %uq_hbm.1, ...), custom_call_target="tpu_custom_call" | custom-call | tf_op jit(solution)/shard_map/pallas_call | solution.py:615
  36.6 0.8 %copy.17 = bf16[64,4096]{1,0:T(8,128)(2,1)} copy(bf16[64,4096]{1,0:T(8,128)(2,1)S(1)} %shard_map.145) | data formatting | bytes 1048576

commit v3 on v2

--- a/solution.py
+++ b/solution.py
@@ -86,9 +86,12 @@
     uqt,
     urt,
     uvt,
-    keys,
-    vals,
-    rots,
+    keys0,
+    vals0,
+    rots0,
+    keys1,
+    vals1,
+    rots1,
     scored,
     load_sem,
     kv_send,
@@ -101,6 +104,7 @@
     cross_recv,
 ):
     O = S // 2
+    keys, vals, rots = (keys0, keys1), (vals0, vals1), (rots0, rots1)
     rows = tokens.shape[0]
     span = rows * T
     depth = tokens.shape[1]
@@ -227,10 +231,11 @@
             def _():
                 kv_copy(o, i_, g_, dev((o + d) % O, i, g, c), O + d - 1).start()
 
+        own = g_ is g
         for d in reversed(range(1, O)):
-            send(d, (o > 0) | (d == O - 1))
+            send(d, ((o > 0) & own) | ((o == 0) & (d == O - 1)))
         for d in range(1, O - 1):
-            send(d, (o == 0) & ((d != O - 2) | (O < 4) | (g_ is not g)))
+            send(d, (o == 0) & ((d != O - 2) | (O < 4)) if own else o < O)
 
     def relay_column(d):
         @pl.when((d == O - 1) & (O >= 4))
@@ -322,13 +327,13 @@
         lat = latents(s)
 
         def key_part(n):
-            keys[slot, :, n : n + wide] = dot(lat, uk[:, n : n + wide]).astype(BF16)
+            keys[slot][:, n : n + wide] = dot(lat, uk[:, n : n + wide]).astype(BF16)
 
         def value_part(n):
-            vals[slot, n : n + wide, :] = dot_nt(uvt[n : n + wide, :], lat).astype(BF16)
+            vals[slot][n : n + wide, :] = dot_nt(uvt[n : n + wide, :], lat).astype(BF16)
 
         def rotary_part():
-            rots[slot] = rotaries(s)
+            rots[slot][...] = rotaries(s)
 
         parts = [functools.partial(key_part, n) for n in range(0, heads * NOPE, wide)]
         parts += [functools.partial(value_part, n) for n in range(0, heads * VDIM, wide)]
@@ -371,15 +376,19 @@
     q_copy(other, mate).wait_recv()
     q_copy(other, mate).start()
 
+    last = (o == O - 1) & (o >= 3)
+
     def seq(j):
-        return sp - j - jnp.where(i == 1, 0, 2 * (j % 2) - 1)
+        m = j + 1 - i
+        d = m // 2
+        d = jnp.where(last & (d >= 2), jnp.where(d == 2, o, d - 1), d)
+        return (o - d) * 2 + jnp.where(m % 2 == 0, i, 1 - i)
 
     @pl.when(i == 1)
     def _():
         mate_in(seq(1))
         kv_heads(seq(1), 1)
 
-    pl.when((o >= 1) & (o == O - 1))(lambda: across_in(1))
     for copy in table_loads:
         copy.wait()
     q_cos = jnp.concatenate([qbase[:HALF, :]] * (span // LANES), axis=1)
@@ -409,52 +418,83 @@
                 qt[n, h] = whole[:, n * side : (n + 1) * side]
 
     def score(slot, h, group):
-        key = jnp.concatenate([keys[slot, :, h * NOPE : (h + 1) * NOPE], rots[slot]], axis=1)
+        key = jnp.concatenate([keys[slot][:, h * NOPE : (h + 1) * NOPE], rots[slot][...]], axis=1)
         return dot(key, qt[group, h])
 
     def attend(slot, group, first=False, ahead=None):
         ones = jnp.ones((acc.shape[1] - VDIM, span), BF16)
-        parts = [] if ahead is None else head_parts(*ahead)
+        parts = [[] for _ in range(heads)]
+        if ahead is not None:
+            todo = head_parts(ahead, 1 - slot)
+            for n, part in enumerate(todo):
+                parts[max(n - len(todo) + heads, 0)].append(part)
         if first:
             k_pos = lax.broadcasted_iota(jnp.int32, (span, side), 0)
             q_pos = lax.broadcasted_iota(jnp.int32, (span, side), 1) + group * side
             allowed = k_pos <= q_pos
+
+        def weigh(h, scores):
+            if first:
+                scores = jnp.where(allowed, scores, masked_score)
+            new = jnp.max(scores, axis=0, keepdims=True)
+            shrink = None
+            if not first:
+                old = best[h][:1]
+                new = jnp.maximum(old, new)
+                shrink = jnp.exp2(old - new)
+            best[h] = jnp.broadcast_to(new, best.shape[1:])
+            return jnp.exp2(scores - new).astype(BF16), shrink
+
+        def gather(h, weights, shrink):
+            value = jnp.concatenate([vals[slot][h * VDIM : (h + 1) * VDIM, :], ones], axis=0)
+            if first:
+                acc[h] = dot(value, weights)
+            else:
+                acc[h] = acc[h] * shrink + dot(value, weights)
+
         later = score(slot, 0, group) if first else scored[...]
+        weighed = None
         for h in range(heads):
             scores = later
             if h + 1 < heads:
                 later = score(slot, h + 1, group)
-            for part in parts[h * len(parts) // heads : (h + 1) * len(parts) // heads]:
+            elif ahead is not None:
+                later = score(1 - slot, 0, group)
+            for part in parts[h]:
                 part()
-            value = jnp.concatenate([vals[slot, h * VDIM : (h + 1) * VDIM, :], ones], axis=0)
-            if first:
-                scores = jnp.where(allowed, scores, masked_score)
-            new = jnp.max(scores, axis=0, keepdims=True)
-            if not first:
-                old = best[h][:1]
-                new = jnp.maximum(old, new)
-            weights = jnp.exp2(scores - new).astype(BF16)
-            if first:
-                acc[h] = dot(value, weights)
-            else:
-                acc[h] = acc[h] * jnp.exp2(old - new) + dot(value, weights)
-            best[h] = jnp.broadcast_to(new, best.shape[1:])
+            now = weigh(h, scores)
+            if weighed is not None:
+                gather(h - 1, *weighed)
+            weighed = now
         if ahead is not None:
-            scored[...] = score(ahead[1], 0, group)
+            scored[...] = later
+        gather(heads - 1, *weighed)
 
     def sweep(group, arriving):
+        def one(j, slot):
+            if arriving:
+                early = (i == 0) | ((o < O - 1) & (j >= 2))
+                pl.when(early & (j + 2 <= sp))(lambda: relay_in(seq(j + 2)))
+                mate_in(seq(j + 1))
+            attend(slot, group, ahead=seq(j + 1))
+            if arriving:
+                pl.when((i == 1) & (o < O - 1) & (j == 1) & (sp >= 3))(lambda: relay_in(seq(3)))
+                pl.when((i == 1) & (o == O - 1) & (j + 3 <= sp))(lambda: relay_in(seq(j + 3)))
+
         @pl.when(sp >= 1)
         def _():
-            def both(j):
-                if arriving:
-                    pl.when((i == 0) & (j + 2 <= sp))(lambda: relay_in(seq(j + 2)))
-                    mate_in(seq(j + 1))
-                attend(j % 2, group, ahead=(seq(j + 1), (j + 1) % 2))
-                if arriving:
-                    pl.when((i == 1) & (j + 3 <= sp))(lambda: relay_in(seq(j + 3)))
-
-            each(1, sp, both)
-            attend(sp % 2, group)
+            def two(n):
+                one(2 * n + 1, 1)
+                one(2 * n + 2, 0)
+
+            each(0, (sp - 1) // 2, two)
+
+            @pl.when(i == 0)
+            def _():
+                one(sp - 1, 1)
+                attend(0, group)
+
+            pl.when(i == 1)(lambda: attend(1, group))
 
         @phase
         def _():
@@ -463,6 +503,7 @@
                 part = (whole[:VDIM] / whole[VDIM : VDIM + 1]).T.astype(BF16)
                 att[pl.ds(pl.multiple_of(group * side, side), side), h * VDIM : (h + 1) * VDIM] = part
 
+    pl.when((o >= 1) & (o == O - 1))(lambda: across_in(1))
     phase(lambda: attend(0, 1 - g, first=True))
 
     @pl.when((o >= 1) & (o < O - 1))
@@ -470,19 +511,17 @@
         each(2, o + 1, column_in)
         across_in(1)
 
-    @pl.when(o >= 1)
+    @pl.when((i == 0) & (o >= 1))
+    def _():
+        mate_in(seq(1))
+        kv_heads(seq(1), 1)
+
+    pl.when(sp >= 1)(lambda: scored.__setitem__(..., score(1, 0, 1 - g)))
+
+    @pl.when((o >= 1) & ((i == 0) | (o == O - 1)))
     def _():
         beside_in(1)
         corner_in(1)
-
-    @pl.when(sp >= 1)
-    def _():
-        @pl.when(i == 0)
-        def _():
-            mate_in(seq(1))
-            kv_heads(seq(1), 1)
-
-        phase(lambda: scored.__setitem__(..., score(1, 0, 1 - g)))
 
     sweep(1 - g, True)
 
@@ -637,9 +676,12 @@
                 pltpu.VMEM(uq.shape[::-1], BF16),
                 pltpu.VMEM(ur.shape[::-1], BF16),
                 pltpu.VMEM(uv.shape[::-1], BF16),
-                pltpu.VMEM((2, span, heads * NOPE), BF16),
-                pltpu.VMEM((2, heads * VDIM, span), BF16),
-                pltpu.VMEM((2, span, LANES), BF16),
+                *[
+                    pltpu.VMEM((span, heads * NOPE), BF16),
+                    pltpu.VMEM((heads * VDIM, span), BF16),
+                    pltpu.VMEM((span, LANES), BF16),
+                ]
+                * 2,
                 pltpu.VMEM((span, span // 2), F32),
                 dma(2 * chunks + 13),
                 dma(2 * O),

time: 37.9 us -> 37.1 us (0.979)
  Pallas kernels: 36.6 us -> 36.1 us
    pallas_call x1, Pallas kernels: 36.6 us -> 36.1 us  [local(): pl.pallas_call(functools.partial(kernel, S, T, chunks, pieces), out_shape...]
where the time goes in v3:
time: 37.1 us; the launch traced here: 36.9 us
  Pallas kernels  36.1 us (97%)
  local copies, waits for them, and re-layouts  0.8 us (2%)
    pallas_call x1, Pallas kernels, local(): pl.pallas_call(functools.partial(kernel, S, T, chunks, pieces), out_shape...  36.1 us
    unnamed x1, local copies, waits for them, and re-layouts  0.8 us

profile of v3, /device:TPU:24, one launch (start us, length us, event | category | flops | bytes accessed | tf_op | source)
XLA Modules:
  0.0 36.9 jit_solution(8253087762934477732)
XLA Ops:
  0.0 36.1 %shard_map.145 = bf16[64,4096]{1,0:T(8,128)(2,1)S(1)} custom-call(bf16[64,4096]{1,0:T(8,128)(2,1)} %tokens_hbm.1, bf16[4096,1024]{1,0:T(8,128)(2,1)} %dq_hbm.1, bf16[4096,512]{1,0:T(8,128)(2,1)} %dl_hbm.1, bf16[64,4096]{1,0:T(8,128)(2,1)} %bitcast.3, f32[1,1024]{1,0:T(1,128)} %bitcast.4, f32[1,512]{1,0:T(1,128)} %bitcast.5, bf16[1024,512]{1,0:T(8,128)(2,1)} %uq_hbm.1, ...), custom_call_target="tpu_custom_call" | custom-call | tf_op jit(solution)/shard_map/pallas_call | solution.py:654
  36.1 0.8 %copy.17 = bf16[64,4096]{1,0:T(8,128)(2,1)} copy(bf16[64,4096]{1,0:T(8,128)(2,1)S(1)} %shard_map.145) | data formatting | bytes 1048576

commit v4 on v3

--- a/solution.py
+++ b/solution.py
@@ -242,7 +242,9 @@
         def _():
             kv_copy(o - d, i, g, dev(O - 2, i, g, c), d).start()
 
-        kv_copy(o - d, i, g, across, d).start()
+        @pl.when(d != 1)
+        def _():
+            kv_copy(o - d, i, g, across, d).start()
 
         @pl.when((i == 0) | (d > 0))
         def _():
@@ -358,12 +360,19 @@
     def _():
         kv_copy(o, i, 1 - g, beside, 2 * O - 1).start()
 
-    pl.when((o >= 1) & (o == O - 1))(lambda: column_in(1))
+    @pl.when(o < O - 1)
+    def _():
+        kv_copy(o, i, 1 - g, dev((o + 1) % O, i, g, c), O).start()
+
+    def own_heads():
+        mate_in(sp)
+        kv_heads(sp, 0)
+
+    pl.when(o == O - 1)(lambda: each(1, o + 1, column_in))
     pl.when(i == 1)(lambda: beside_in(0))
     uqt[...] = uq[...].T
     urt[...] = ur[...].T
-    mate_in(sp)
-    phase(lambda: kv_heads(sp, 0))
+    pl.when(o < O - 1)(own_heads)
 
     @pl.when((i == 1) | (o < O - 1))
     def _():
@@ -371,10 +380,9 @@
         up(1 - g, 1 - i)
 
     pl.when((o >= 1) & (o < O - 1))(lambda: column_in(1))
-
-    pl.when(o == O - 1)(lambda: each(2, o + 1, column_in))
     q_copy(other, mate).wait_recv()
     q_copy(other, mate).start()
+    pl.when(o == O - 1)(own_heads)
 
     last = (o == O - 1) & (o >= 3)
 
@@ -595,12 +603,19 @@
     pl.when(i == 1)(lambda: kv_blocks(5, 0, 0).wait_send())
     pl.when((i == 0) | (o < O - 1))(lambda: kv_blocks(1, 2 * O - 1, 0).wait_send())
 
-    def some_sent(few, count, index):
-        pl.when(few)(lambda: kv_blocks(count - 1, index, 0).wait_send())
-        pl.when(jnp.logical_not(few))(lambda: kv_blocks(count, index, 0).wait_send())
-
-    each(1, o + 1, lambda d: some_sent((d < O - 1) | (O < 4), 7, d))
-    each(1, O - o, lambda d: some_sent((o == 0) & (d == O - 2) & (O >= 4), 2, O + d - 1))
+    def counted(index, count, counts):
+        for n in counts:
+            pl.when(count == n)(lambda n=n: kv_blocks(n, index, 0).wait_send())
+
+    def relays_sent(d):
+        counted(d, 6 - jnp.where(d == 1, 1, 0) + jnp.where((d == O - 1) & (O >= 4), 1, 0), (5, 6, 7))
+
+    def ups_sent(d):
+        skipped = (o == 0) & (d == O - 2) & (O >= 4)
+        counted(O + d - 1, 2 + jnp.where(d == 1, 1, 0) - jnp.where(skipped, 1, 0), (1, 2, 3))
+
+    each(1, o + 1, relays_sent)
+    each(1, O - o, ups_sent)
     all_sent(ql.at[pl.ds(0, 3 * rows)], q_send)
     all_sent(pair_out, pair_send)
     pltpu.make_async_remote_copy(

time: 37.1 us -> 37.1 us (level)
  no operation moved by 1% of the time
where the time goes in v4:
time: 37.1 us; the launch traced here: 36.9 us
  Pallas kernels  36.1 us (97%)
  local copies, waits for them, and re-layouts  0.8 us (2%)
    pallas_call x1, Pallas kernels, local(): pl.pallas_call(functools.partial(kernel, S, T, chunks, pieces), out_shape...  36.1 us
    unnamed x1, local copies, waits for them, and re-layouts  0.8 us

profile of v4, /device:TPU:24, one launch (start us, length us, event | category | flops | bytes accessed | tf_op | source)
XLA Modules:
  0.0 36.9 jit_solution(2838995654446398889)
XLA Ops:
  0.0 36.1 %shard_map.145 = bf16[64,4096]{1,0:T(8,128)(2,1)S(1)} custom-call(bf16[64,4096]{1,0:T(8,128)(2,1)} %tokens_hbm.1, bf16[4096,1024]{1,0:T(8,128)(2,1)} %dq_hbm.1, bf16[4096,512]{1,0:T(8,128)(2,1)} %dl_hbm.1, bf16[64,4096]{1,0:T(8,128)(2,1)} %bitcast.3, f32[1,1024]{1,0:T(1,128)} %bitcast.4, f32[1,512]{1,0:T(1,128)} %bitcast.5, bf16[1024,512]{1,0:T(8,128)(2,1)} %uq_hbm.1, ...), custom_call_target="tpu_custom_call" | custom-call | tf_op jit(solution)/shard_map/pallas_call | solution.py:669
  36.1 0.8 %copy.17 = bf16[64,4096]{1,0:T(8,128)(2,1)} copy(bf16[64,4096]{1,0:T(8,128)(2,1)S(1)} %shard_map.145) | data formatting | bytes 1048576

commit v5 on v4

--- a/solution.py
+++ b/solution.py
@@ -535,7 +535,7 @@
 
     ow_load.wait()
     width = ow.shape[1] // pieces
-    lag = min(3, pieces)
+    lag = min(5, pieces)
 
     def pair_copy(second, j):
         return pltpu.make_async_remote_copy(
@@ -643,7 +643,7 @@
         heads = uk.shape[1] // NOPE
         width = ow.shape[1]
         rank = dl.shape[1]
-        chunks, pieces = 4, 8
+        chunks, pieces = 4, 16
         inverse = np.float32(rope_base) ** (-np.arange(0, ROPE, 2, dtype=np.float32) / np.float32(ROPE))
         inverse = inverse.astype(np.float64)
         tiled = np.tile(inverse, LANES // HALF)

time: 37.1 us -> 37.1 us (level)
  no operation moved by 1% of the time
where the time goes in v5:
time: 37.1 us; the launch traced here: 36.9 us
  Pallas kernels  36.1 us (97%)
  local copies, waits for them, and re-layouts  0.8 us (2%)
    pallas_call x1, Pallas kernels, local(): pl.pallas_call(functools.partial(kernel, S, T, chunks, pieces), out_shape...  36.1 us
    unnamed x1, local copies, waits for them, and re-layouts  0.8 us

profile of v5, /device:TPU:24, one launch (start us, length us, event | category | flops | bytes accessed | tf_op | source)
XLA Modules:
  0.0 36.9 jit_solution(14912306933404686423)
XLA Ops:
  0.0 36.1 %shard_map.145 = bf16[64,4096]{1,0:T(8,128)(2,1)S(1)} custom-call(bf16[64,4096]{1,0:T(8,128)(2,1)} %tokens_hbm.1, bf16[4096,1024]{1,0:T(8,128)(2,1)} %dq_hbm.1, bf16[4096,512]{1,0:T(8,128)(2,1)} %dl_hbm.1, bf16[64,4096]{1,0:T(8,128)(2,1)} %bitcast.3, f32[1,1024]{1,0:T(1,128)} %bitcast.4, f32[1,512]{1,0:T(1,128)} %bitcast.5, bf16[1024,512]{1,0:T(8,128)(2,1)} %uq_hbm.1, ...), custom_call_target="tpu_custom_call" | custom-call | tf_op jit(solution)/shard_map/pallas_call | solution.py:669
  36.1 0.8 %copy.17 = bf16[64,4096]{1,0:T(8,128)(2,1)} copy(bf16[64,4096]{1,0:T(8,128)(2,1)S(1)} %shard_map.145) | data formatting | bytes 1048576
